TPU v7x, 32 devices: a whole 2x2x4 slice. The times are simulated.
32 devices in a mesh: fs: 8 (over z, y), tp: 4 (over x, core).
Axes of the slice: x: 2, y: 2, z: 4, core: 2. Of those that a mesh axis runs over, the one named last changes fastest.
Arguments:
- tokens: bfloat16 [4096, 2048], P(('fs', 'tp')), may hold values from -6 to 6
- pre_gain: float32 [2048], replicated, may hold values from 0.1 to 1.9
- w_expand: bfloat16 [2048, 8192], P('fs', 'tp'), may hold values from -0.125 to 0.125
- w_reduce: bfloat16 [8192, 2048], P('tp', 'fs'), may hold values from -0.0625 to 0.0625
- post_gain: float32 [2048], replicated, may hold values from 0.1 to 1.9
Outputs:
- result: bfloat16 [4096, 2048], P(('fs', 'tp'))
All inputs are finite; a program needn't handle non-finite values.
Results may differ from a plain program's by a relative error of at most 0.014.
Values may be sent and summed in bfloat16 or wider, within the bound.
A program may use at most 64 MiB of HBM per device.

v0:
```python
import jax
import jax.numpy as jnp
from jax import lax
from jax.sharding import PartitionSpec as P

NORM_EPS = 1e-06


def rms_scale(values, gain_row):
    widened = values.astype(jnp.float32)
    scaled = widened * lax.rsqrt(jnp.mean(widened * widened, axis=-1, keepdims=True) + NORM_EPS)
    return scaled * gain_row


def squared_relu(preact):
    return jnp.square(jnp.maximum(preact, 0.0)).astype(jnp.bfloat16)


def per_device(tokens, pre_gain, w_expand, w_reduce, post_gain):
    normed = rms_scale(tokens, pre_gain).astype(jnp.bfloat16)
    expand_full = lax.all_gather(w_expand, "fs", axis=0, tiled=True)
    hidden = squared_relu(
        jnp.dot(
            lax.all_gather(normed, "tp", axis=0, tiled=True),
            expand_full,
            preferred_element_type=jnp.float32,
        )
    )
    reduce_full = lax.all_gather(w_reduce, "fs", axis=1, tiled=True)
    mixed = lax.psum_scatter(
        jnp.dot(hidden, reduce_full, preferred_element_type=jnp.float32).astype(jnp.bfloat16),
        "tp",
        scatter_dimension=0,
        tiled=True,
    )
    return rms_scale(mixed, post_gain).astype(jnp.bfloat16)


def solution(mesh):
    return jax.shard_map(
        per_device,
        mesh=mesh,
        in_specs=(P(("fs", "tp"), None), P(), P("fs", "tp"), P("tp", "fs"), P()),
        out_specs=P(("fs", "tp"), None),
        check_vma=False,
    )
```

profile of v0, /device:TPU:0, one launch (start us, length us, event | category | flops | bytes accessed | tf_op | source)
XLA Modules:
  0.0 342.9 jit_solution(1764702396853761959)
XLA Ops:
  6.5 0.0 all-gather.4.cloned.1.call-start
  6.5 1.2 fusion
  7.8 2.0 fusion.2
  9.8 0.0 all-gather.4.cloned.1.call-update
  9.8 0.0 all-gather.6.cloned.1.call-start
  9.9 0.7 all-gather.6.cloned.1.call-update
  10.6 0.0 all-gather.8.cloned.1.call-start
  10.6 0.7 all-gather.8.cloned.1.call-update
  11.3 0.0 copy-start
  11.3 0.0 reduce-scatter.2.cloned.1.call-start
  11.4 23.9 %all-gather.4.cloned.1.call-done = bf16[512,2048]{1,0:T(8,128)(2,1)} async-done(((bf16[128,2048]{1,0:T(8,128)(2,1)}), bf16[512,2048]{1,0:T(8,128)(2,1)}) %all-gather.4.cloned.1.call-update) | async-done | bytes 2097168 | tf_op jit(solution)/shard_map/all_gather | solution.py:24
  35.3 126.6 %all-gather.6.cloned.1.call-done = bf16[2048,2048]{1,0:T(8,128)(2,1)} async-done(((bf16[256,2048]{1,0:T(8,128)(2,1)}), bf16[2048,2048]{1,0:T(8,128)(2,1)}) %all-gather.6.cloned.1.call-update) | async-done | bytes 8388624 | tf_op jit(solution)/shard_map/all_gather | solution.py:21
  161.9 125.2 %all-gather.8.cloned.1.call-done = bf16[2048,2048]{1,0:T(8,128)(2,1)} async-done(((bf16[2048,256]{1,0:T(8,128)(2,1)}), bf16[2048,2048]{1,0:T(8,128)(2,1)}) %all-gather.8.cloned.1.call-update) | async-done | bytes 8388624 | tf_op jit(solution)/shard_map/all_gather | solution.py:29
  287.1 16.5 %convolution_convert_fusion = bf16[512,2048]{1,0:T(8,128)(2,1)} fusion(bf16[2048,2048]{1,0:T(8,128)(2,1)} %all-gather.8.cloned.1.call-done, bf16[512,2048]{1,0:T(8,128)(2,1)} %all-gather.4.cloned.1.call-done, bf16[2048,2048]{1,0:T(8,128)(2,1)} %all-gather.6.cloned.1.call-done), kind=kOutput, calls=%fused_computation.1 | convolution fusion | flops 8594128896 | bytes 20971520 | tf_op jit(solution)/shard_map/dot_general | solution.py:31
  303.6 0.0 reduce-scatter.2.cloned.1.call-update
  303.6 29.5 %reduce-scatter.2.cloned.1.call-done = bf16[128,2048]{1,0:T(8,128)(2,1)} async-done(((bf16[512,2048]{1,0:T(8,128)(2,1)}), bf16[128,2048]{1,0:T(8,128)(2,1)}) %reduce-scatter.2.cloned.1.call-update) | async-done | bytes 524304 | tf_op jit(solution)/shard_map/reduce_scatter | solution.py:30
  333.1 1.2 fusion.3
  334.4 0.0 copy-done
  334.4 2.0 fusion.5
  (2 shorter events, 0.0 us)
Async XLA Ops:
  6.5 28.7 %all-gather.4.cloned.1.call-start = ((), (), s32[]{:S(2)}) async-start(), calls=%async_computation.1 | async-start | bytes 2621440 | tf_op jit(solution)/shard_map/all_gather | solution.py:24
  9.8 152.1 %all-gather.6.cloned.1.call-start = ((), (), s32[]{:S(2)}) async-start(), calls=%async_computation.2 | async-start | bytes 9437184 | tf_op jit(solution)/shard_map/all_gather | solution.py:21
  10.6 276.5 %all-gather.8.cloned.1.call-start = ((), (), s32[]{:S(2)}) async-start(), calls=%async_computation.3 | async-start | bytes 9437184 | tf_op jit(solution)/shard_map/all_gather | solution.py:29
  11.3 323.0 %copy-start = (f32[2048]{0:T(1024)S(1)}, f32[2048]{0:T(1024)}, u32[]{:S(2)}) copy-start(f32[2048]{0:T(1024)} %param.9) | copy-start | bytes 24580
  11.3 321.8 %reduce-scatter.2.cloned.1.call-start = ((), (), s32[]{:S(2)}) async-start(), calls=%async_computation.4 | async-start | bytes 2621440 | tf_op jit(solution)/shard_map/reduce_scatter | solution.py:30
Sparse Core Ops, SparseCore 0:
  9.9 25.2 all-gather.3
  37.4 124.4 all-gather.5
  164.0 123.1 all-gather.7
  303.8 29.3 reduce-scatter.1
where the time goes:
time: 343 us
  waiting for transfers between devices  307 us (90%)
  matrix products  16.5 us (5%)
  between operations  13.1 us (4%)
  other arithmetic  6.53 us (2%)
    all_gather x1, waiting for transfers between devices, per_device(): expand_full = lax.all_gather(w_expand, 'fs', axis=0, tiled=True)  127 us
    all_gather x1, waiting for transfers between devices, per_device(): reduce_full = lax.all_gather(w_reduce, 'fs', axis=1, tiled=True)  125 us
    reduce_scatter x1, waiting for transfers between devices, per_device(): lax.psum_scatter(jnp.dot(hidden, reduce_full, preferred_element_type=jnp....  29.5 us
    all_gather x1, waiting for transfers between devices, per_device(): lax.all_gather(normed, 'tp', axis=0, tiled=True)  23.9 us
    dot_general x1, matrix products, per_device(): jnp.dot(hidden, reduce_full, preferred_element_type=jnp.float32)  16.5 us
  transfers between devices with their start and end apart: 4, of which 4 were waited for; matrix products, arithmetic and copies ran while one was open for 0% of the time, Pallas kernels for 0%

commit v1 on v0

--- a/solution.py
+++ b/solution.py
@@ -18,7 +18,12 @@
 
 def per_device(tokens, pre_gain, w_expand, w_reduce, post_gain):
     normed = rms_scale(tokens, pre_gain).astype(jnp.bfloat16)
-    expand_full = lax.all_gather(w_expand, "fs", axis=0, tiled=True)
+    ring = [w_expand]
+    for hop in range(7):
+        ring.append(lax.ppermute(ring[-1], "fs", [(dev, (dev + 1) % 8) for dev in range(8)]))
+    expand_full = jnp.roll(
+        jnp.concatenate(ring[::-1], axis=0), (lax.axis_index("fs") + 1) * ring[0].shape[0], axis=0
+    )
     hidden = squared_relu(
         jnp.dot(
             lax.all_gather(normed, "tp", axis=0, tiled=True),

time: 343 us -> 372 us (1.085)
  local copies, waits for them, and re-layouts: 0.01 us -> 29 us
  waiting for transfers between devices: 307 us -> 303 us
    ppermute x0 -> x7, waiting for transfers between devices: none -> 270 us  [per_device(): lax.ppermute(ring[-1], 'fs', [(dev, (dev + 1) % 8) for dev in range(8)])]
    all_gather x1 -> x0, waiting for transfers between devices: 127 us -> none  [per_device(): expand_full = lax.all_gather(w_expand, 'fs', axis=0, tiled=True)]
    all_gather x1, waiting for transfers between devices: 125 us -> 0.01 us  [per_device(): reduce_full = lax.all_gather(w_reduce, 'fs', axis=1, tiled=True)]
    unnamed x2 -> x31, local copies, waits for them, and re-layouts: 0.01 us -> 27.9 us
    all_gather x1, waiting for transfers between devices: 23.9 us -> 0.01 us  [per_device(): lax.all_gather(normed, 'tp', axis=0, tiled=True)]
  transfers between devices with their start and end apart: 4 -> 10, of which waited for: 4 -> 8; matrix products, arithmetic and copies ran while one was open for 0% -> 7% of each run, Pallas kernels for 0% -> 0%
where the time goes in v1:
time: 372 us; the launch traced here: 371 us
  waiting for transfers between devices  303 us (81%)
  local copies, waits for them, and re-layouts  29 us (8%)
  matrix products  16.5 us (4%)
  between operations  13.1 us (4%)
  other arithmetic  6.61 us (2%)
    ppermute x7, waiting for transfers between devices, per_device(): lax.ppermute(ring[-1], 'fs', [(dev, (dev + 1) % 8) for dev in range(8)])  270 us
    reduce_scatter x1, waiting for transfers between devices, per_device(): lax.psum_scatter(jnp.dot(hidden, reduce_full, preferred_element_type=jnp....  31.8 us
    unnamed x31, local copies, waits for them, and re-layouts  27.9 us
    dot_general x1, matrix products, per_device(): jnp.dot(hidden, reduce_full, preferred_element_type=jnp.float32)  16.5 us
  transfers between devices with their start and end apart: 10, of which 8 were waited for; matrix products, arithmetic and copies ran while one was open for 7% of the time, Pallas kernels for 0%

profile of v1, /device:TPU:0, one launch (start us, length us, event | category | flops | bytes accessed | tf_op | source)
XLA Modules:
  0.0 371.3 jit_solution(9016899625961913129)
XLA Ops:
  6.5 1.3 fusion.4
  7.9 2.0 fusion.6
  10.7 3.0 collective-permute-start
  13.8 26.4 %collective-permute-done = bf16[256,2048]{1,0:T(8,128)(2,1)S(1)} collective-permute-done((bf16[256,2048]{1,0:T(8,128)(2,1)}, bf16[256,2048]{1,0:T(8,128)(2,1)S(1)}, u32[]{:S(2)}, u32[]{:S(2)}) %collective-permute-start) | collective-permute-done | bytes 1048608 | tf_op jit(solution)/shard_map/ppermute | solution.py:23
  40.2 42.9 %collective-permute-done.1 = bf16[256,2048]{1,0:T(8,128)(2,1)S(1)} collective-permute-done((bf16[256,2048]{1,0:T(8,128)(2,1)S(1)}, bf16[256,2048]{1,0:T(8,128)(2,1)S(1)}, u32[]{:S(2)}, u32[]{:S(2)}) %collective-permute-start.1) | collective-permute-done | bytes 1048608 | tf_op jit(solution)/shard_map/ppermute | solution.py:23
  83.1 40.4 %collective-permute-done.2 = bf16[256,2048]{1,0:T(8,128)(2,1)S(1)} collective-permute-done((bf16[256,2048]{1,0:T(8,128)(2,1)S(1)}, bf16[256,2048]{1,0:T(8,128)(2,1)S(1)}, u32[]{:S(2)}, u32[]{:S(2)}) %collective-permute-start.2) | collective-permute-done | bytes 1048608 | tf_op jit(solution)/shard_map/ppermute | solution.py:23
  124.4 50.3 %collective-permute-done.3 = bf16[256,2048]{1,0:T(8,128)(2,1)S(1)} collective-permute-done((bf16[256,2048]{1,0:T(8,128)(2,1)S(1)}, bf16[256,2048]{1,0:T(8,128)(2,1)S(1)}, u32[]{:S(2)}, u32[]{:S(2)}) %collective-permute-start.3) | collective-permute-done | bytes 1048608 | tf_op jit(solution)/shard_map/ppermute | solution.py:23
  174.8 1.0 copy-done.3
  175.8 50.1 %collective-permute-done.4 = bf16[256,2048]{1,0:T(8,128)(2,1)S(1)} collective-permute-done((bf16[256,2048]{1,0:T(8,128)(2,1)S(1)}, bf16[256,2048]{1,0:T(8,128)(2,1)S(1)}, u32[]{:S(2)}, u32[]{:S(2)}) %collective-permute-start.4) | collective-permute-done | bytes 1048608 | tf_op jit(solution)/shard_map/ppermute | solution.py:23
  225.8 1.0 copy-done.5
  226.9 32.6 %collective-permute-done.5 = bf16[256,2048]{1,0:T(8,128)(2,1)} collective-permute-done((bf16[256,2048]{1,0:T(8,128)(2,1)S(1)}, bf16[256,2048]{1,0:T(8,128)(2,1)}, u32[]{:S(2)}, u32[]{:S(2)}) %collective-permute-start.5) | collective-permute-done | bytes 1048608 | tf_op jit(solution)/shard_map/ppermute | solution.py:23
  259.4 27.8 %collective-permute-done.6 = bf16[256,2048]{1,0:T(8,128)(2,1)} collective-permute-done((bf16[256,2048]{1,0:T(8,128)(2,1)}, bf16[256,2048]{1,0:T(8,128)(2,1)}, u32[]{:S(2)}, u32[]{:S(2)}) %collective-permute-start.6) | collective-permute-done | bytes 1048608 | tf_op jit(solution)/shard_map/ppermute | solution.py:23
  287.2 2.3 constant_dynamic-update-slice_fusion.15
  289.5 2.3 constant_dynamic-update-slice_fusion.14
  291.8 2.3 constant_dynamic-update-slice_fusion.13
  294.2 2.3 constant_dynamic-update-slice_fusion.12
  296.5 2.3 constant_dynamic-update-slice_fusion.11
  298.8 1.1 constant_dynamic-update-slice_fusion.10
  299.9 1.1 constant_dynamic-update-slice_fusion.9
  300.9 1.1 constant_dynamic-update-slice_fusion.8
  302.1 2.4 constant_dynamic-update-slice_fusion.7
  304.5 2.3 constant_dynamic-update-slice_fusion.6
  306.8 1.0 constant_dynamic-update-slice_fusion.5
  307.8 1.1 constant_dynamic-update-slice_fusion.4
  308.9 1.1 constant_dynamic-update-slice_fusion.3
  310.0 1.0 constant_dynamic-update-slice_fusion.2
  311.0 1.1 constant_dynamic-update-slice_fusion.1
  312.1 1.1 constant_dynamic-update-slice_fusion
  313.2 16.5 %convolution_convert_fusion = bf16[512,2048]{1,0:T(8,128)(2,1)} fusion(bf16[2048,2048]{1,0:T(8,128)(2,1)} %all-gather.5.cloned.1.call-done, bf16[512,2048]{1,0:T(8,128)(2,1)} %all-gather.3.cloned.1.call-done, bf16[4096,2048]{1,0:T(8,128)(2,1)} %constant_dynamic-update-slice_fusion, s32[]{:T(128)S(6)} %select_n.14), kind=kOutput, calls=%fused_computation.3 | convolution fusion | flops 8594128896 | bytes 20971524 | tf_op jit(solution)/shard_map/dot_general | solution.py:36
  329.7 31.8 %reduce-scatter.2.cloned.1.call-done = bf16[128,2048]{1,0:T(8,128)(2,1)} async-done(((bf16[512,2048]{1,0:T(8,128)(2,1)}), bf16[128,2048]{1,0:T(8,128)(2,1)}) %reduce-scatter.2.cloned.1.call-update) | async-done | bytes 524304 | tf_op jit(solution)/shard_map/reduce_scatter | solution.py:35
  361.5 1.2 fusion.7
  362.7 2.0 fusion.9
  (30 shorter events, 1.8 us)
Async XLA Ops:
  6.5 294.4 %copy-start = (bf16[256,2048]{1,0:T(8,128)(2,1)S(1)}, bf16[256,2048]{1,0:T(8,128)(2,1)}, u32[]{:S(2)}) copy-start(bf16[256,2048]{1,0:T(8,128)(2,1)} %param.7) | copy-start | bytes 3145732
  6.5 306.6 %all-gather.3.cloned.1.call-start = ((), (), s32[]{:S(2)}) async-start(), calls=%async_computation.1 | async-start | bytes 2621440 | tf_op jit(solution)/shard_map/all_gather | solution.py:29
  9.9 303.3 %all-gather.5.cloned.1.call-start = ((), (), s32[]{:S(2)}) async-start(), calls=%async_computation.2 | async-start | bytes 9437184 | tf_op jit(solution)/shard_map/all_gather | solution.py:34
  10.7 350.8 %reduce-scatter.2.cloned.1.call-start = ((), (), s32[]{:S(2)}) async-start(), calls=%async_computation.3 | async-start | bytes 2621440 | tf_op jit(solution)/shard_map/reduce_scatter | solution.py:35
  10.7 29.5 %collective-permute-start = (bf16[256,2048]{1,0:T(8,128)(2,1)}, bf16[256,2048]{1,0:T(8,128)(2,1)S(1)}, u32[]{:S(2)}, u32[]{:S(2)}) collective-permute-start(bf16[256,2048]{1,0:T(8,128)(2,1)} %param.7), channel_id=1, source_target_pairs={{0,4},{4,8},{8,12},{12,16},{16,20},{20,24},{24,28},{28,0},{1,5},{5... | collective-permute-start | bytes 3145736 | tf_op jit(solution)/shard_map/ppermute | solution.py:23
  40.2 42.9 %collective-permute-start.1 = (bf16[256,2048]{1,0:T(8,128)(2,1)S(1)}, bf16[256,2048]{1,0:T(8,128)(2,1)S(1)}, u32[]{:S(2)}, u32[]{:S(2)}) collective-permute-start(bf16[256,2048]{1,0:T(8,128)(2,1)S(1)} %collective-permute-done), channel_id=1, source_target_pairs={{0,4},{4,8},{8,12},{12,16},{16,20},{20,24},{24,28},{28,0},{1,5},{5... | collective-permute-start | bytes 3145736 | tf_op jit(solution)/shard_map/ppermute | solution.py:23
  83.1 40.4 %collective-permute-start.2 = (bf16[256,2048]{1,0:T(8,128)(2,1)S(1)}, bf16[256,2048]{1,0:T(8,128)(2,1)S(1)}, u32[]{:S(2)}, u32[]{:S(2)}) collective-permute-start(bf16[256,2048]{1,0:T(8,128)(2,1)S(1)} %collective-permute-done.1), channel_id=1, source_target_pairs={{0,4},{4,8},{8,12},{12,16},{16,20},{20,24},{24,28},{28,0},{1,5},{5... | collective-permute-start | bytes 3145736 | tf_op jit(solution)/shard_map/ppermute | solution.py:23
  123.5 1.0 copy-start.1
  124.4 50.3 %collective-permute-start.3 = (bf16[256,2048]{1,0:T(8,128)(2,1)S(1)}, bf16[256,2048]{1,0:T(8,128)(2,1)S(1)}, u32[]{:S(2)}, u32[]{:S(2)}) collective-permute-start(bf16[256,2048]{1,0:T(8,128)(2,1)S(1)} %collective-permute-done.2), channel_id=1, source_target_pairs={{0,4},{4,8},{8,12},{12,16},{16,20},{20,24},{24,28},{28,0},{1,5},{5... | collective-permute-start | bytes 3145736 | tf_op jit(solution)/shard_map/ppermute | solution.py:23
  174.7 1.0 copy-start.3
  175.7 50.1 %collective-permute-start.4 = (bf16[256,2048]{1,0:T(8,128)(2,1)S(1)}, bf16[256,2048]{1,0:T(8,128)(2,1)S(1)}, u32[]{:S(2)}, u32[]{:S(2)}) collective-permute-start(bf16[256,2048]{1,0:T(8,128)(2,1)S(1)} %collective-permute-done.3), channel_id=1, source_target_pairs={{0,4},{4,8},{8,12},{12,16},{16,20},{20,24},{24,28},{28,0},{1,5},{5... | collective-permute-start | bytes 3145736 | tf_op jit(solution)/shard_map/ppermute | solution.py:23
  225.8 1.1 copy-start.5
  226.9 32.6 %collective-permute-start.5 = (bf16[256,2048]{1,0:T(8,128)(2,1)S(1)}, bf16[256,2048]{1,0:T(8,128)(2,1)}, u32[]{:S(2)}, u32[]{:S(2)}) collective-permute-start(bf16[256,2048]{1,0:T(8,128)(2,1)S(1)} %collective-permute-done.4), channel_id=1, source_target_pairs={{0,4},{4,8},{8,12},{12,16},{16,20},{20,24},{24,28},{28,0},{1,5},{5... | collective-permute-start | bytes 3145736 | tf_op jit(solution)/shard_map/ppermute | solution.py:23
  259.4 27.8 %collective-permute-start.6 = (bf16[256,2048]{1,0:T(8,128)(2,1)}, bf16[256,2048]{1,0:T(8,128)(2,1)}, u32[]{:S(2)}, u32[]{:S(2)}) collective-permute-start(bf16[256,2048]{1,0:T(8,128)(2,1)} %collective-permute-done.5), channel_id=1, source_target_pairs={{0,4},{4,8},{8,12},{12,16},{16,20},{20,24},{24,28},{28,0},{1,5},{5... | collective-permute-start | bytes 3145736 | tf_op jit(solution)/shard_map/ppermute | solution.py:23
  259.4 47.3 %copy-start.6 = (bf16[256,2048]{1,0:T(8,128)(2,1)S(1)}, bf16[256,2048]{1,0:T(8,128)(2,1)}, u32[]{:S(2)}) copy-start(bf16[256,2048]{1,0:T(8,128)(2,1)} %copy-done.5) | copy-start | bytes 3145732
  259.4 48.4 %copy-start.4 = (bf16[256,2048]{1,0:T(8,128)(2,1)S(1)}, bf16[256,2048]{1,0:T(8,128)(2,1)}, u32[]{:S(2)}) copy-start(bf16[256,2048]{1,0:T(8,128)(2,1)} %copy-done.3) | copy-start | bytes 3145732
  259.4 49.4 %copy-start.2 = (bf16[256,2048]{1,0:T(8,128)(2,1)S(1)}, bf16[256,2048]{1,0:T(8,128)(2,1)}, u32[]{:S(2)}) copy-start(bf16[256,2048]{1,0:T(8,128)(2,1)} %copy-done.1) | copy-start | bytes 3145732
  313.2 49.6 %copy-start.7 = (f32[2048]{0:T(1024)S(1)}, f32[2048]{0:T(1024)}, u32[]{:S(2)}) copy-start(f32[2048]{0:T(1024)} %param.9) | copy-start | bytes 24580
Sparse Core Ops, SparseCore 0:
  10.0 25.2 all-gather.2
  37.4 192.9 all-gather.4
  329.8 31.6 reduce-scatter.1
